TPU v7x, 32 devices: a whole 2x2x4 slice. The times are simulated.
32 devices in a mesh: sp: 8 (over z, x), tp: 4 (over y, core).
Axes of the slice: x: 2, y: 2, z: 4, core: 2. Of those that a mesh axis runs over, the one named last changes fastest.
Arguments:
- residual: bfloat16 [1536, 2048], P(('sp', 'tp')), may hold values from -6 to 6
- query_a: bfloat16 [1536, 1536], P('sp', 'tp'), may hold values from -600 to 600
- query_b: bfloat16 [1536, 2560], P('sp', 'tp'), may hold values from -600 to 600
- latents: bfloat16 [1536, 512], P('sp'), may hold values from -6 to 6
- rope_key: bfloat16 [1536, 32], P('sp'), may hold values from -6 to 6
- key_up_a: bfloat16 [512, 1024], P(None, 'tp'), may hold values from -0.25 to 0.25
- value_up_a: bfloat16 [512, 1024], P(None, 'tp'), may hold values from -0.25 to 0.25
- key_up_b: bfloat16 [512, 2048], P(None, 'tp'), may hold values from -0.25 to 0.25
- value_up_b: bfloat16 [512, 2048], P(None, 'tp'), may hold values from -0.25 to 0.25
- out_proj_a: bfloat16 [1024, 2048], P('tp'), may hold values from -1.5 to 1.5
- out_proj_b: bfloat16 [2048, 2048], P('tp'), may hold values from -1.5 to 1.5
- norm_gain: float32 [2048], replicated, may hold values from 0.1 to 1.9
- routes: int32 [1536, 2], P('sp'), may hold values from 0 to 7, all different within a row; in each aligned block of 192 rows (0 to 191, 192 to 383, ...) at most 72 rows name the same one
- route_weights: float32 [1536, 2], P('sp'), may hold values from 0.2 to 1
- shared_gate: bfloat16 [2048, 2048], P(None, 'tp'), may hold values from -0.125 to 0.125
- shared_up: bfloat16 [2048, 2048], P(None, 'tp'), may hold values from -0.125 to 0.125
- shared_down: bfloat16 [2048, 2048], P('tp'), may hold values from -0.125 to 0.125
- expert_gate: bfloat16 [8, 2048, 2048], P('sp', None, 'tp'), may hold values from -0.125 to 0.125
- expert_up: bfloat16 [8, 2048, 2048], P('sp', None, 'tp'), may hold values from -0.125 to 0.125
- expert_down: bfloat16 [8, 2048, 2048], P('sp', 'tp'), may hold values from -0.125 to 0.125
Outputs:
- layer_out: bfloat16 [1536, 2048], P(('sp', 'tp'))
Inputs may be any that keep to these rules, and one draw needn't show every extreme that they name: `routes`: in each aligned block of 192 rows, no expert is named by more than 72 rows, a bound that some block reaches; a row names 2 different experts.
All inputs are finite; a program needn't handle non-finite values.
Results may differ from a plain program's by a relative error of at most 0.022.
The roundings to bfloat16 on the way count: a program that leaves them out, or rounds other values in their place, can miss the bound.
Values may be sent and summed in bfloat16 or wider, within the bound.
No kernel may reach another device: no remote copies, remote signals or barrier semaphores. Data moves between devices by JAX's collectives and lax.ppermute only.
A program may use at most 64 MiB of HBM per device.

v0:
```python
import jax
import jax.numpy as jnp
from jax import lax
from jax.sharding import PartitionSpec as P

DA = 64
VA = 64
DB = 128
VB = 128
ROPE = 32


theta_base = 10000.0
norm_eps = 1e-06
very_low = -1e30


def tables(positions, width):
    half = width // 2
    freqs = theta_base ** (-(2.0 * jnp.arange(half, dtype=jnp.float32)) / width)
    angles = positions.astype(jnp.float32)[:, None] * freqs[None, :]
    return (jnp.cos(angles), jnp.sin(angles))


def rotate(values, cosine, sine):
    half = values.shape[-1] // 2
    first = values[..., :half].astype(jnp.float32)
    second = values[..., half:].astype(jnp.float32)
    turned = jnp.concatenate(
        [first * cosine - second * sine, first * sine + second * cosine], axis=-1
    )
    return turned.astype(jnp.bfloat16)


def group_update(state, queries_nope, queries_rope, keys, values, rot_piece, mask, scale):
    top, total, weighted = state
    scores = jnp.einsum("qhd,khd->hqk", queries_nope, keys, preferred_element_type=jnp.float32)
    scores = scores + jnp.einsum(
        "qhr,kr->hqk", queries_rope, rot_piece, preferred_element_type=jnp.float32
    )
    scores = jnp.where(mask[None], scores * scale, very_low)
    new_top = jnp.maximum(top, jnp.max(scores, axis=-1))
    expo = jnp.where(mask[None], jnp.exp(scores - new_top[..., None]), 0.0)
    total = jnp.sum(expo, axis=-1)
    weighted = jnp.einsum(
        "hqk,khv->hqv", expo.astype(jnp.bfloat16), values, preferred_element_type=jnp.float32
    )
    return (new_top, total, weighted)


def empty_state(heads, rows, vsize):
    return (
        jnp.full((heads, rows), very_low, jnp.float32),
        jnp.zeros((heads, rows), jnp.float32),
        jnp.zeros((heads, rows, vsize), jnp.float32),
    )


def shards(
    residual,
    query_a,
    query_b,
    latents,
    rope_key,
    key_up_a,
    value_up_a,
    key_up_b,
    value_up_b,
    out_proj_a,
    out_proj_b,
    norm_gain,
    routes,
    route_weights,
    shared_gate,
    shared_up,
    shared_down,
    expert_gate,
    expert_up,
    expert_down,
):
    tok = query_a.shape[0]
    heads_a = key_up_a.shape[1] // DA
    heads_b = key_up_b.shape[1] // DB
    first_row = lax.axis_index("sp") * tok
    last_row = first_row + tok
    query_pos = first_row + jnp.arange(tok, dtype=jnp.int32)
    cosine, sine = tables(query_pos, ROPE)
    rot_key = rotate(rope_key, cosine, sine)
    shaped_a = query_a.reshape(tok, heads_a, DA + ROPE)
    shaped_b = query_b.reshape(tok, heads_b, DB + ROPE)
    nope_a = shaped_a[..., :DA]
    nope_b = shaped_b[..., :DB]
    turned_a = rotate(shaped_a[..., DA:], cosine[:, None, :], sine[:, None, :])
    turned_b = rotate(shaped_b[..., DB:], cosine[:, None, :], sine[:, None, :])
    scale_a = (DA + ROPE) ** (-0.5)
    scale_b = (DB + ROPE) ** (-0.5)

    def attend(state, keys_a, values_a, keys_b, values_b, rot_piece, key_pos):
        count = keys_a.shape[0]
        mask = key_pos[None, :] <= query_pos[:, None]
        state_a = group_update(
            state[0],
            nope_a,
            turned_a,
            keys_a.reshape(count, heads_a, DA),
            values_a.reshape(count, heads_a, VA),
            rot_piece,
            mask,
            scale_a,
        )
        state_b = group_update(
            state[1],
            nope_b,
            turned_b,
            keys_b.reshape(count, heads_b, DB),
            values_b.reshape(count, heads_b, VB),
            rot_piece,
            mask,
            scale_b,
        )
        return (state_a, state_b)

    def project_latents(lat_rows):
        keys_a = jnp.dot(lat_rows, key_up_a, preferred_element_type=jnp.float32).astype(
            jnp.bfloat16
        )
        values_a = jnp.dot(lat_rows, value_up_a, preferred_element_type=jnp.float32).astype(
            jnp.bfloat16
        )
        keys_b = jnp.dot(lat_rows, key_up_b, preferred_element_type=jnp.float32).astype(
            jnp.bfloat16
        )
        values_b = jnp.dot(lat_rows, value_up_b, preferred_element_type=jnp.float32).astype(
            jnp.bfloat16
        )
        return (keys_a, values_a, keys_b, values_b)

    start_state = (empty_state(heads_a, tok, VA), empty_state(heads_b, tok, VB))
    lat_rows = lax.all_gather(latents, "sp", axis=0, tiled=True)
    rot_piece = lax.all_gather(rot_key, "sp", axis=0, tiled=True)
    key_pos = jnp.arange(lat_rows.shape[0], dtype=jnp.int32)

    def compute(inner):
        keys_a, values_a, keys_b, values_b = project_latents(lat_rows)
        return attend(inner, keys_a, values_a, keys_b, values_b, rot_piece, key_pos)

    state = lax.cond(jnp.int32(0) < last_row, compute, lambda inner: inner, start_state)
    heads_out_a = (state[0][2] / state[0][1][..., None]).astype(jnp.bfloat16)
    heads_out_b = (state[1][2] / state[1][1][..., None]).astype(jnp.bfloat16)
    proj_a = out_proj_a.reshape(heads_a, VA, out_proj_a.shape[1])
    proj_b = out_proj_b.reshape(heads_b, VB, out_proj_b.shape[1])
    term = jnp.einsum("hqv,hvd->qd", heads_out_a, proj_a, preferred_element_type=jnp.float32)
    mixed = lax.psum_scatter(
        (
            term
            + jnp.einsum("hqv,hvd->qd", heads_out_b, proj_b, preferred_element_type=jnp.float32)
        ).astype(jnp.bfloat16),
        "tp",
        scatter_dimension=0,
        tiled=True,
    ).astype(jnp.float32)
    hidden_state = (residual.astype(jnp.float32) + mixed).astype(jnp.bfloat16)
    wide = hidden_state.astype(jnp.float32)
    normed = (
        wide * lax.rsqrt(jnp.mean(wide * wide, axis=-1, keepdims=True) + norm_eps) * norm_gain
    ).astype(jnp.bfloat16)
    whole_rows = lax.all_gather(normed, "tp", axis=0, tiled=True)
    shared_act = (
        jax.nn.silu(jnp.dot(whole_rows, shared_gate, preferred_element_type=jnp.float32))
        * jnp.dot(whole_rows, shared_up, preferred_element_type=jnp.float32)
    ).astype(jnp.bfloat16)
    experts = lax.axis_size("sp")
    topk = routes.shape[1]
    capacity = max(2, 3 * tok * topk // (2 * experts))
    flat = routes.reshape(-1)
    onehot = (flat[:, None] == jnp.arange(experts, dtype=jnp.int32)[None, :]).astype(jnp.int32)
    before = jnp.cumsum(onehot, axis=0) - onehot
    rank = jnp.sum(before * onehot, axis=1)
    slots = (flat * capacity + rank).reshape(tok, topk)
    placing = jnp.sum(
        (
            slots[:, :, None] == jnp.arange(experts * capacity, dtype=jnp.int32)[None, None, :]
        ).astype(jnp.bfloat16),
        axis=1,
    )
    outgoing = jnp.einsum(
        "rs,rd->sd", placing, whole_rows, preferred_element_type=jnp.float32
    ).astype(jnp.bfloat16)
    outgoing = outgoing.reshape(experts, capacity, whole_rows.shape[1])
    gate_w = expert_gate[0]
    up_w = expert_up[0]
    down_w = expert_down[0]
    arrived = lax.all_to_all(outgoing, "sp", split_axis=0, concat_axis=0, tiled=True)
    sources, items, width = arrived.shape
    rows_in = arrived.reshape(sources * items, width)
    act = (
        jax.nn.silu(jnp.dot(rows_in, gate_w, preferred_element_type=jnp.float32))
        * jnp.dot(rows_in, up_w, preferred_element_type=jnp.float32)
    ).astype(jnp.bfloat16)
    part = jnp.dot(act, down_w, preferred_element_type=jnp.float32).astype(jnp.bfloat16)
    back = lax.all_to_all(
        part.reshape(sources, items, down_w.shape[1]), "sp", split_axis=0, concat_axis=0, tiled=True
    )
    back_flat = back.reshape(experts * capacity, back.shape[2])
    term = jnp.dot(shared_act, shared_down, preferred_element_type=jnp.float32)
    picked = jnp.take(back_flat, slots, axis=0).astype(jnp.float32)
    moe = lax.psum_scatter(
        (term + jnp.sum(picked * route_weights[..., None], axis=1)).astype(jnp.bfloat16),
        "tp",
        scatter_dimension=0,
        tiled=True,
    ).astype(jnp.float32)
    return (hidden_state.astype(jnp.float32) + moe).astype(jnp.bfloat16)


def solution(mesh):
    placed = (
        P(("sp", "tp"), None),
        P("sp", "tp"),
        P("sp", "tp"),
        P("sp", None),
        P("sp", None),
        P(None, "tp"),
        P(None, "tp"),
        P(None, "tp"),
        P(None, "tp"),
        P("tp", None),
        P("tp", None),
        P(),
        P("sp", None),
        P("sp", None),
        P(None, "tp"),
        P(None, "tp"),
        P("tp", None),
        P("sp", None, "tp"),
        P("sp", None, "tp"),
        P("sp", "tp", None),
    )
    return jax.shard_map(
        shards, mesh=mesh, in_specs=placed, out_specs=P(("sp", "tp"), None), check_vma=False
    )
```

profile of v0, /device:TPU:0, one launch (start us, length us, event | category | flops | bytes accessed | tf_op | source)
XLA Modules:
  0.0 296.8 jit_solution(13761831657723779826)
XLA Ops:
  10.4 32.5 %all-gather = bf16[8,192,32]{1,2,0:T(8,128)(2,1)S(1)} all-gather(bf16[1,192,32]{1,2,0:T(8,128)(2,1)S(1)} %maximum_bitcast_fusion), channel_id=1, replica_groups=mesh['sp'=8,'tp'=4] {'sp'}, dimensions={0}, use_global_device_ids=true | all-gather | bytes 110592 | tf_op jit(solution)/shard_map/all_gather | solution.py:140
  43.0 13.4 %all-gather.3.cloned.1.call-done = bf16[1536,512]{1,0:T(8,128)(2,1)} async-done(((bf16[192,512]{1,0:T(8,128)(2,1)}), bf16[1536,512]{1,0:T(8,128)(2,1)}) %all-gather.3.cloned.1.call-update) | async-done | bytes 1572880 | tf_op jit(solution)/shard_map/all_gather | solution.py:139
  57.0 19.7 %conditional.1 = (f32[4,192]{1,0:T(4,128)S(1)}, f32[4,192,64]{1,2,0:T(8,128)S(1)}, f32[4,192]{1,0:T(4,128)S(1)}, f32[4,192,128]{2,1,0:T(8,128)S(1)}) conditional(s32[]{:T(128)} %convert_element_type.111, () %tuple.13, (s32[1536]{0:T(1024)S(1)}, s32[]{:T(128)}, s32[192]{0:T(256)}, bf16[1536,512]{1,0:T(8,128)(2,1)}, bf16[512,256]{1,0:T(8,128)(2,1)}, ...), branch_computations={%region_0.0_spmd, %region_1.6_spmd} | conditional | flops 3499129600 | bytes 87277032 | solution.py:147
  57.3 2.9 fusion.20
  60.2 2.2 convolution_convert_fusion.1
  62.9 4.1 %fusion.75 = (f32[4,192]{1,0:T(4,128)S(1)}, f32[4,192,1536]{2,1,0:T(8,128)S(1)}) fusion(f32[1536,192,4]{0,1,2:T(8,128)} %fusion.20, bf16[1536,4,128]{0,2,1:T(8,128)(2,1)} %bitcast.102, bf16[192,4,160]{2,0,1:T(8,128)(2,1)S(1)} %copy.83, pred[192,1536]{1,0:T(8,128)(4,1)S(1)} %broadcast_compare_fusion), kind=kOutput, calls=%fused_computation.123 | convolution fusion | flops 306707712 | bytes 11504640 | tf_op jit(solution)/shard_map/cond/branch_1_fun/qhd,khd->hqk/dot_general | solution.py:37
  69.1 1.6 fusion.76
  70.7 2.3 fusion.7
  76.7 1.6 convolution_bitcast_fusion
  78.4 1.6 fusion.27
  82.1 19.8 %reduce-scatter.3.cloned.1.call-done = bf16[48,2048]{1,0:T(8,128)(2,1)} async-done(((bf16[192,2048]{1,0:T(8,128)(2,1)}), bf16[48,2048]{1,0:T(8,128)(2,1)}) %reduce-scatter.3.cloned.1.call-update) | async-done | bytes 196624 | tf_op jit(solution)/shard_map/reduce_scatter | solution.py:153
  104.1 8.2 %all_gather.11 = bf16[192,2048]{1,0:T(8,128)(2,1)S(1)} all-gather(bf16[48,2048]{1,0:T(8,128)(2,1)S(1)} %fusion.48), channel_id=1, replica_groups=mesh['sp'=8,'tp'=4] {'tp'}, dimensions={0}, use_global_device_ids=true | all-gather | bytes 983040 | tf_op jit(solution)/shard_map/all_gather | solution.py:167
  113.1 59.7 %all_to_all.10 = bf16[8,72,2048]{2,1,0:T(8,128)(2,1)S(1)} all-to-all(bf16[8,72,2048]{2,1,0:T(8,128)(2,1)S(1)} %bitcast.95), channel_id=1, replica_groups=mesh['sp'=8,'tp'=4] {'sp'}, dimensions={0} | all-to-all | bytes 4718592 | tf_op jit(solution)/shard_map/all_to_all | solution.py:193
  174.3 2.4 fusion.32
  176.7 7.4 %convolution_convert_fusion.4 = bf16[576,2048]{1,0:T(8,128)(2,1)} fusion(bf16[1,512,2048]{2,1,0:T(8,128)(2,1)} %param.41, bf16[576,2048]{1,0:T(8,128)(2,1)} %bitcast.99, bf16[1,2048,512]{2,1,0:T(8,128)(2,1)} %param.40, f32[576,512]{1,0:T(8,128)} %fusion.32), kind=kOutput, calls=%fused_computation.39 | convolution fusion | flops 2418868224 | bytes 10092544 | tf_op jit(solution)/shard_map/dot_general | solution.py:200
  184.1 4.5 %all-to-all-start.1 = ((bf16[8,72,2048]{2,1,0:T(8,128)(2,1)}), bf16[8,72,2048]{2,1,0:T(8,128)(2,1)}, u32[]{:S(2)}, u32[]{:S(2)}) async-start(bf16[8,72,2048]{2,1,0:T(8,128)(2,1)} %bitcast.97), calls=%async_computation.2 | async-start | bytes 4718592 | tf_op jit(solution)/shard_map/all_to_all | solution.py:201
  189.3 2.9 fusion.77
  192.2 49.9 %all-to-all-done.1 = bf16[8,72,2048]{2,1,0:T(8,128)(2,1)} async-done(((bf16[8,72,2048]{2,1,0:T(8,128)(2,1)}), bf16[8,72,2048]{2,1,0:T(8,128)(2,1)}, u32[]{:S(2)}, u32[]{:S(2)}) %all-to-all-start.1) | async-done | bytes 2359328 | tf_op jit(solution)/shard_map/all_to_all | solution.py:201
  242.1 7.0 %gather_fusion = bf16[384,2048]{1,0:T(8,128)(2,1)} fusion(bf16[576,2048]{1,0:T(8,128)(2,1)} %bitcast.24, s32[1024]{0:T(1024)S(1)} %pad_clamp_fusion), kind=kCustom, calls=%fused_computation | custom fusion | bytes 3147264 | tf_op jit(solution)/shard_map/jit(_take)/gather | solution.py:206
  249.2 3.8 %reshape.181 = bf16[192,2,2048]{2,1,0:T(2,128)(2,1)} reshape(bf16[384,2048]{1,0:T(8,128)(2,1)} %gather_fusion) | data formatting | bytes 3145728 | tf_op jit(solution)/shard_map/jit(_take)/gather | solution.py:206
  252.9 8.7 %multiply_reduce_fusion = f32[192,2048]{1,0:T(8,128)} fusion(bf16[192,2,2048]{2,1,0:T(2,128)(2,1)} %reshape.181, pred[192,2]{1,0:T(8,128)(4,1)S(1)} %copy.87, f32[192,2]{1,0:T(8,128)S(1)} %copy.89), kind=kLoop, calls=%fused_computation.37 | loop fusion | flops 2752512 | bytes 3147648 | tf_op jit(solution)/shard_map/reduce_sum | solution.py:208
  261.7 4.8 %fusion.28 = bf16[192,2048]{1,0:T(8,128)(2,1)} fusion(f32[192,2048]{1,0:T(8,128)} %multiply_reduce_fusion, bf16[512,2048]{1,0:T(8,128)(2,1)} %param.38, bf16[192,2048]{1,0:T(8,128)(2,1)S(1)} %all_gather.11, bf16[2048,512]{1,0:T(8,128)(2,1)} %param.37, f32[192,512]{1,0:T(8,128)} %fusion.77), kind=kOutput, calls=%fused_computation.46 | convolution fusion | flops 806682624 | bytes 7733248 | tf_op jit(solution)/shard_map/dot_general | solution.py:205
  266.5 22.0 %reduce-scatter.5.cloned.1.call-done = bf16[48,2048]{1,0:T(8,128)(2,1)} async-done(((bf16[192,2048]{1,0:T(8,128)(2,1)}), bf16[48,2048]{1,0:T(8,128)(2,1)}) %reduce-scatter.5.cloned.1.call-update) | async-done | bytes 196624 | tf_op jit(solution)/shard_map/reduce_scatter | solution.py:207
  288.6 1.7 fusion.49
  (80 shorter events, 17.8 us)
Async XLA Ops:
  6.5 71.8 %copy-start = (bf16[512,2048]{1,0:T(8,128)(2,1)S(1)}, bf16[512,2048]{1,0:T(8,128)(2,1)}, u32[]{:S(2)}) copy-start(bf16[512,2048]{1,0:T(8,128)(2,1)} %param.32) | copy-start | bytes 6291460
  6.5 49.9 %all-gather.3.cloned.1.call-start = ((), (), s32[]{:S(2)}) async-start(), calls=%async_computation.4 | async-start | bytes 1769472 | tf_op jit(solution)/shard_map/all_gather | solution.py:139
  7.3 94.6 %reduce-scatter.3.cloned.1.call-start = ((), (), s32[]{:S(2)}) async-start(), calls=%async_computation.5 | async-start | bytes 983040 | tf_op jit(solution)/shard_map/reduce_scatter | solution.py:153
  57.3 3.0 %copy-start.1 = (bf16[1536,512]{1,0:T(8,128)(2,1)S(1)}, bf16[1536,512]{1,0:T(8,128)(2,1)}, u32[]{:S(2)}) copy-start(bf16[1536,512]{1,0:T(8,128)(2,1)} %get-tuple-element.38) | copy-start | bytes 4718596 | tf_op jit(solution)/shard_map/cond
  57.3 3.0 copy-start.13
  60.2 2.4 copy-start.11
  67.0 1.4 copy-start.2
  67.0 1.4 copy-start.6
  70.7 2.4 copy-start.7
  73.7 1.1 copy-start.14
  78.4 1.6 copy-start.9
  78.4 23.5 %copy-start.4 = (bf16[48,2048]{1,0:T(8,128)(2,1)S(1)}, bf16[48,2048]{1,0:T(8,128)(2,1)}, u32[]{:S(2)}) copy-start(bf16[48,2048]{1,0:T(8,128)(2,1)} %param.22) | copy-start | bytes 589828
  78.4 24.6 %copy-start.8 = (f32[2048]{0:T(1024)S(1)}, f32[2048]{0:T(1024)}, u32[]{:S(2)}) copy-start(f32[2048]{0:T(1024)} %param.33) | copy-start | bytes 24580
  113.1 61.2 %copy-start.12 = (bf16[1,2048,512]{2,1,0:T(8,128)(2,1)S(1)}, bf16[1,2048,512]{2,1,0:T(8,128)(2,1)}, u32[]{:S(2)}) copy-start(bf16[1,2048,512]{2,1,0:T(8,128)(2,1)} %param.39) | copy-start | bytes 6291460
  172.9 1.4 copy-start.3
  184.1 5.0 %copy-start.10 = (f32[192,2]{0,1:T(2,128)S(1)}, f32[192,2]{0,1:T(2,128)}, u32[]{:S(2)}) copy-start(f32[192,2]{0,1:T(2,128)} %param.35) | copy-start | bytes 4612
  184.1 58.0 %all-to-all-start.1 = ((bf16[8,72,2048]{2,1,0:T(8,128)(2,1)}), bf16[8,72,2048]{2,1,0:T(8,128)(2,1)}, u32[]{:S(2)}, u32[]{:S(2)}) async-start(bf16[8,72,2048]{2,1,0:T(8,128)(2,1)} %bitcast.97), calls=%async_computation.2 | async-start | bytes 4718592 | tf_op jit(solution)/shard_map/all_to_all | solution.py:201
  188.6 100.0 %reduce-scatter.5.cloned.1.call-start = ((), (), s32[]{:S(2)}) async-start(), calls=%async_computation.6 | async-start | bytes 983040 | tf_op jit(solution)/shard_map/reduce_scatter | solution.py:207
  261.7 26.9 %copy-start.5 = (bf16[48,2048]{1,0:T(8,128)(2,1)S(1)}, bf16[48,2048]{1,0:T(8,128)(2,1)}, u32[]{:S(2)}) copy-start(bf16[48,2048]{1,0:T(8,128)(2,1)} %reduce-scatter.3.cloned.1.call-done) | copy-start | bytes 589828
Sparse Core Ops, SparseCore 0:
  9.5 46.9 all-gather.2
  80.1 21.7 reduce-scatter.2
  266.7 21.8 reduce-scatter.4
where the time goes:
time: 297 us
  waiting for transfers between devices  106 us (36%)
  blocking collectives  101 us (34%)
  matrix products  37.6 us (13%)
  local copies, waits for them, and re-layouts  17.4 us (6%)
  other arithmetic  17.3 us (6%)
  between operations  13.3 us (4%)
  starting transfers between devices  4.59 us (2%)
    all_to_all x1, blocking collectives, shards(): lax.all_to_all(outgoing, 'sp', split_axis=0, concat_axis=0, tiled=True)  59.7 us
    all_to_all x1, waiting for transfers between devices, shards(): lax.all_to_all(part.reshape(sources, items, down_w.shape[1]), 'sp', split...  49.9 us
    all_gather x1, blocking collectives, shards(): rot_piece = lax.all_gather(rot_key, 'sp', axis=0, tiled=True)  32.5 us
    reduce_scatter x1, waiting for transfers between devices, shards(): lax.psum_scatter((term + jnp.sum(picked * route_weights[..., None], axis=...  22 us
    reduce_scatter x1, waiting for transfers between devices, shards(): lax.psum_scatter((term + jnp.einsum('hqv,hvd->qd', heads_out_b, proj_b, p...  19.8 us
    all_gather x1, waiting for transfers between devices, shards(): lat_rows = lax.all_gather(latents, 'sp', axis=0, tiled=True)  13.4 us
    gather x2, local copies, waits for them, and re-layouts, shards(): picked = jnp.take(back_flat, slots, axis=0).astype(jnp.float32)  10.8 us
    reduce_sum x1, other arithmetic, shards(): jnp.sum(picked * route_weights[..., None], axis=1)  8.74 us
  transfers between devices with their start and end apart: 4, of which 4 were waited for; matrix products, arithmetic and copies ran while one was open for 3% of the time, Pallas kernels for 0%

commit v1 on v0

v1 whole, which is shorter than its diff:
```python
import functools

import jax
import jax.numpy as jnp
from jax import lax
from jax.experimental import pallas as pl
from jax.experimental.pallas import tpu as pltpu
from jax.sharding import PartitionSpec as P

DA = 64
VA = 64
DB = 128
VB = 128
ROPE = 32


theta_base = 10000.0
norm_eps = 1e-06
very_low = -1e30


def tables(positions, width):
    half = width // 2
    freqs = theta_base ** (-(2.0 * jnp.arange(half, dtype=jnp.float32)) / width)
    angles = positions.astype(jnp.float32)[:, None] * freqs[None, :]
    return (jnp.cos(angles), jnp.sin(angles))


def rotate(values, cosine, sine):
    half = values.shape[-1] // 2
    first = values[..., :half].astype(jnp.float32)
    second = values[..., half:].astype(jnp.float32)
    turned = jnp.concatenate(
        [first * cosine - second * sine, first * sine + second * cosine], axis=-1
    )
    return turned.astype(jnp.bfloat16)


def head_kernel(
    qa_ref, qb_ref, lat_ref, rota_ref, rotb_ref, kua_ref, vua_ref, kub_ref, vub_ref,
    qpos_ref, kpos_ref, out_ref, *, scale_a, scale_b
):
    mask = kpos_ref[...] <= qpos_ref[...]
    lat = lat_ref[...]

    def attend(queries, keys, values, scale):
        scores = lax.dot_general(
            queries, keys, (((1,), (1,)), ((), ())), preferred_element_type=jnp.float32
        )
        scores = jnp.where(mask, scores, very_low)
        top = jnp.max(scores, axis=-1, keepdims=True)
        expo = jnp.exp((scores - top) * scale)
        total = jnp.sum(expo, axis=-1, keepdims=True)
        weighted = jnp.dot(expo.astype(jnp.bfloat16), values, preferred_element_type=jnp.float32)
        return (weighted / total).astype(jnp.bfloat16)

    def project(weights):
        return jnp.dot(lat, weights, preferred_element_type=jnp.float32).astype(jnp.bfloat16)

    wide_a = kua_ref.shape[2]
    wide_v = vua_ref.shape[2]
    count_a = qa_ref.shape[0]
    for h in range(count_a):
        keys = project(kua_ref[h]) + rota_ref[...]
        out_ref[:, h * wide_v : (h + 1) * wide_v] = attend(
            qa_ref[h], keys, project(vua_ref[h]), scale_a
        )
    base = count_a * wide_v
    wide_k = kub_ref.shape[1] // qb_ref.shape[0]
    wide_v = vub_ref.shape[1] // qb_ref.shape[0]
    for h in range(qb_ref.shape[0]):
        keys = project(kub_ref[:, h * wide_k : (h + 1) * wide_k])
        keys = jnp.concatenate([keys, rotb_ref[...]], axis=1)
        out_ref[:, base + h * wide_v : base + (h + 1) * wide_v] = attend(
            qb_ref[h], keys, project(vub_ref[:, h * wide_v : (h + 1) * wide_v]), scale_b
        )


def padded_heads(weights, heads, lanes):
    split = weights.reshape(weights.shape[0], heads, -1)
    split = jnp.pad(split, ((0, 0), (0, 0), (0, lanes - split.shape[2])))
    return jnp.transpose(split, (1, 0, 2))


def swap(values, axis, b):
    return lax.ppermute(values, axis, [(i, i ^ (1 << b)) for i in range(lax.axis_size(axis))])


def join(values, axis, b, dim):
    other = swap(values, axis, b)
    low = ((lax.axis_index(axis) >> b) & 1) == 0
    return jnp.concatenate(
        [jnp.where(low, values, other), jnp.where(low, other, values)], axis=dim
    )


def shards(
    residual,
    query_a,
    query_b,
    latents,
    rope_key,
    key_up_a,
    value_up_a,
    key_up_b,
    value_up_b,
    out_proj_a,
    out_proj_b,
    norm_gain,
    routes,
    route_weights,
    shared_gate,
    shared_up,
    shared_down,
    expert_gate,
    expert_up,
    expert_down,
):
    tok = query_a.shape[0]
    heads_a = key_up_a.shape[1] // DA
    heads_b = key_up_b.shape[1] // DB
    width = residual.shape[1]
    columns = Columns(width)
    sp_bits = lax.axis_size("sp").bit_length() - 1
    tp_bits = lax.axis_size("tp").bit_length() - 1

    rank = latents.shape[1]
    lanes = rank // lax.axis_size("tp")
    half = tok // 2
    piece = lax.dynamic_slice_in_dim(latents, columns.block * lanes, lanes, 1)
    packed = rope_key.reshape(tok * ROPE // lanes, lanes)
    one = jnp.concatenate([piece[:half], packed], axis=0)[None]
    two = piece[None, half:]
    order = list(range(1, sp_bits)) + [0]
    for b in order[:-1]:
        one = join(one, "sp", b, 0)
        two = join(two, "sp", b, 0)
    one = join(one, "sp", 0, 0)
    rope_rows = one[:, half:].reshape(-1, ROPE)
    one = one[:, :half]
    for b in reversed(range(1, tp_bits)):
        two = join(two, "tp", b, 2)
        one = join(one, "tp", b, 2)
    two = join(two, "sp", 0, 0)
    one = join(one, "tp", 0, 2)
    two = join(two, "tp", 0, 2)
    lat_rows = jnp.concatenate([one, two], axis=1).reshape(-1, rank)
    blocks = jnp.arange(lax.axis_size("sp"), dtype=jnp.int32)
    blocks = sum(((blocks >> j) & 1) << b for j, b in enumerate(order))
    key_pos = (blocks[:, None] * tok + jnp.arange(tok, dtype=jnp.int32)[None, :]).reshape(-1)

    query_pos = lax.axis_index("sp") * tok + jnp.arange(tok, dtype=jnp.int32)
    cosine, sine = tables(query_pos, ROPE)
    shaped_a = query_a.reshape(tok, heads_a, DA + ROPE)
    shaped_b = query_b.reshape(tok, heads_b, DB + ROPE)
    turned_a = rotate(shaped_a[..., DA:], cosine[:, None, :], sine[:, None, :])
    turned_b = rotate(shaped_b[..., DB:], cosine[:, None, :], sine[:, None, :])
    wide_a = -(-(DA + ROPE) // 128) * 128
    wide_v = -(-VA // 128) * 128
    extra = -(-ROPE // 128) * 128 - ROPE
    whole_a = jnp.concatenate([shaped_a[..., :DA], turned_a], axis=2)
    whole_a = jnp.pad(whole_a, ((0, 0), (0, 0), (0, wide_a - DA - ROPE)))
    whole_b = jnp.concatenate([shaped_b[..., :DB], turned_b], axis=2)
    whole_b = jnp.pad(whole_b, ((0, 0), (0, 0), (0, extra)))
    all_cos, all_sin = tables(key_pos, ROPE)
    rot_piece = rotate(rope_rows, all_cos, all_sin)
    heads_out = pl.pallas_call(
        functools.partial(
            head_kernel, scale_a=(DA + ROPE) ** (-0.5), scale_b=(DB + ROPE) ** (-0.5)
        ),
        out_shape=jax.ShapeDtypeStruct((tok, heads_a * wide_v + heads_b * VB), jnp.bfloat16),
        compiler_params=pltpu.CompilerParams(vmem_limit_bytes=56 * 1024 * 1024),
    )(
        jnp.transpose(whole_a, (1, 0, 2)),
        jnp.transpose(whole_b, (1, 0, 2)),
        lat_rows,
        jnp.pad(rot_piece, ((0, 0), (DA, wide_a - DA - ROPE))),
        jnp.pad(rot_piece, ((0, 0), (0, extra))),
        padded_heads(key_up_a, heads_a, wide_a),
        padded_heads(value_up_a, heads_a, wide_v),
        key_up_b,
        value_up_b,
        query_pos[:, None],
        key_pos[None, :],
    )
    proj_a = out_proj_a.reshape(heads_a, VA, width)
    proj_a = jnp.pad(proj_a, ((0, 0), (0, wide_v - VA), (0, 0))).reshape(-1, width)
    proj = jnp.concatenate([proj_a, out_proj_b], axis=0)
    term = jnp.dot(heads_out, proj, preferred_element_type=jnp.float32).astype(jnp.bfloat16)
    mixed = columns.reduce(term)
    hidden_state = (columns.from_rows(residual).astype(jnp.float32) + mixed).astype(jnp.bfloat16)
    hidden = hidden_state.astype(jnp.float32)
    square = jnp.sum(hidden * hidden, axis=-1, keepdims=True)
    for b in range(tp_bits):
        square = square + swap(square, "tp", b)
    gain = lax.dynamic_slice_in_dim(norm_gain, columns.block * columns.size, columns.size, 0)
    normed = (hidden * lax.rsqrt(square / width + norm_eps) * gain).astype(jnp.bfloat16)
    whole_rows = columns.gather(normed)

    experts = lax.axis_size("sp")
    topk = routes.shape[1]
    capacity = max(2, 3 * tok * topk // (2 * experts))
    padded = -(-capacity // 8) * 8
    flat = routes.reshape(-1)
    onehot = (flat[:, None] == jnp.arange(experts, dtype=jnp.int32)[None, :]).astype(jnp.int32)
    before = jnp.cumsum(onehot, axis=0) - onehot
    rank = jnp.sum(before * onehot, axis=1)
    slots = (flat * padded + rank).reshape(tok, topk)
    places = jnp.arange(experts * padded, dtype=jnp.int32)
    chosen = [(slots[:, k, None] == places[None, :]).astype(jnp.bfloat16) for k in range(topk)]
    placing = sum(chosen[1:], chosen[0])

    outgoing = jnp.dot(placing.T, normed, preferred_element_type=jnp.float32)
    outgoing = outgoing.astype(jnp.bfloat16).reshape(experts, padded, columns.size)
    arrived = lax.all_to_all(outgoing, "sp", split_axis=0, concat_axis=0, tiled=True)
    rows_in = columns.gather(arrived.reshape(experts * padded, columns.size))
    shared_act = (
        jax.nn.silu(jnp.dot(whole_rows, shared_gate, preferred_element_type=jnp.float32))
        * jnp.dot(whole_rows, shared_up, preferred_element_type=jnp.float32)
    ).astype(jnp.bfloat16)
    shared_term = jnp.dot(shared_act, shared_down, preferred_element_type=jnp.float32)
    shared_own = columns.reduce(shared_term)
    act = (
        jax.nn.silu(jnp.dot(rows_in, expert_gate[0], preferred_element_type=jnp.float32))
        * jnp.dot(rows_in, expert_up[0], preferred_element_type=jnp.float32)
    ).astype(jnp.bfloat16)
    part = jnp.dot(act, expert_down[0], preferred_element_type=jnp.float32).astype(jnp.bfloat16)
    summed = columns.reduce(part).astype(jnp.bfloat16)
    back = lax.all_to_all(
        summed.reshape(experts, padded, columns.size), "sp", split_axis=0, concat_axis=0, tiled=True
    ).reshape(experts * padded, columns.size)
    moe = shared_own
    for k in range(topk):
        picked = jnp.dot(chosen[k], back, preferred_element_type=jnp.float32)
        moe = moe + picked * route_weights[:, k, None]
    return columns.to_rows((hidden + moe).astype(jnp.bfloat16))


class Columns:
    def __init__(self, width):
        count = lax.axis_size("tp")
        self.count = count
        self.bits = count.bit_length() - 1
        self.size = width // count
        self.index = lax.axis_index("tp")
        self.block = sum(
            ((self.index >> b) & 1) << (self.bits - 1 - b) for b in range(self.bits)
        )

    def of(self, device):
        return sum(((device >> b) & 1) << (self.bits - 1 - b) for b in range(self.bits))

    def gather(self, values):
        for b in reversed(range(self.bits)):
            values = join(values, "tp", b, 1)
        return values

    def reduce(self, values):
        for b in range(self.bits):
            half = values.shape[1] // 2
            bit = (self.index >> b) & 1
            first, second = values[:, :half], values[:, half:]
            sent = jnp.where(bit == 0, second, first).astype(jnp.bfloat16)
            kept = jnp.where(bit == 0, first, second).astype(jnp.float32)
            values = kept + swap(sent, "tp", b).astype(jnp.float32)
        return values

    def trade(self, piece_for, step):
        pairs = [(i, i ^ step) for i in range(self.count)]
        piece = piece_for(self.index ^ step)
        return piece if step == 0 else lax.ppermute(piece, "tp", pairs)

    def from_rows(self, values):
        rows = values.shape[0]
        result = jnp.zeros((rows * self.count, self.size), values.dtype)
        for step in range(self.count):
            piece = self.trade(
                lambda d: lax.dynamic_slice_in_dim(values, self.of(d) * self.size, self.size, 1),
                step,
            )
            result = lax.dynamic_update_slice_in_dim(result, piece, (self.index ^ step) * rows, 0)
        return result

    def to_rows(self, values):
        rows = values.shape[0] // self.count
        result = jnp.zeros((rows, self.size * self.count), values.dtype)
        for step in range(self.count):
            piece = self.trade(lambda d: lax.dynamic_slice_in_dim(values, d * rows, rows, 0), step)
            start = self.of(self.index ^ step) * self.size
            result = lax.dynamic_update_slice_in_dim(result, piece, start, 1)
        return result


def solution(mesh):
    placed = (
        P(("sp", "tp"), None),
        P("sp", "tp"),
        P("sp", "tp"),
        P("sp", None),
        P("sp", None),
        P(None, "tp"),
        P(None, "tp"),
        P(None, "tp"),
        P(None, "tp"),
        P("tp", None),
        P("tp", None),
        P(),
        P("sp", None),
        P("sp", None),
        P(None, "tp"),
        P(None, "tp"),
        P("tp", None),
        P("sp", None, "tp"),
        P("sp", None, "tp"),
        P("sp", "tp", None),
    )
    return jax.shard_map(
        shards, mesh=mesh, in_specs=placed, out_specs=P(("sp", "tp"), None), check_vma=False
    )
```

time: 297 us -> 206 us (0.69)
  blocking collectives: 101 us -> 20.4 us
  waiting for transfers between devices: 106 us -> 51.7 us
  starting transfers between devices: 4.59 us -> 31.5 us
  local copies, waits for them, and re-layouts: 17.4 us -> 35.9 us
  matrix products: 37.6 us -> 20.3 us
  Pallas kernels: 0 us -> 15.3 us
  between operations: 13.3 us -> 0.7 us
  other arithmetic: 17.3 us -> 28.6 us
    ppermute x0 -> x28, waiting for transfers between devices: none -> 43.2 us  [the longest x22 39.7 us: swap(): lax.ppermute(values, axis, [(i, i ^ 1 << b) for i in range(lax.axis_size(...]
    reduce_scatter x2 -> x0, waiting for transfers between devices: 41.9 us -> none  [the longest x1 22 us: shards(): lax.psum_scatter((term + jnp.sum(picked * route_weights[..., None], axis=...]
    all_to_all x1, waiting for transfers between devices: 49.9 us -> 8.51 us  [shards(): lax.all_to_all(summed.reshape(experts, padded, columns.size), 'sp', split...]
    all_gather x2 -> x0, blocking collectives: 40.8 us -> none  [the longest x1 32.5 us: shards(): rot_piece = lax.all_gather(rot_key, 'sp', axis=0, tiled=True)]
    all_to_all x1, blocking collectives: 59.7 us -> 20.4 us  [shards(): lax.all_to_all(outgoing, 'sp', split_axis=0, concat_axis=0, tiled=True)]
    ppermute x0 -> x28, starting transfers between devices: none -> 27.1 us  [the longest x22 23.2 us: swap(): lax.ppermute(values, axis, [(i, i ^ 1 << b) for i in range(lax.axis_size(...]
    dot_general x17 -> x8, matrix products: 37.6 us -> 20.3 us  [the longest x1 6.41 us: shards(): jnp.dot(act, expert_down[0], preferred_element_type=jnp.float32)]
    pallas_call x0 -> x1, Pallas kernels: none -> 15.3 us  [shards(): pl.pallas_call(functools.partial(head_kernel, scale_a=(DA + ROPE) ** (-0....]
  transfers between devices with their start and end apart: 4 -> 29, of which waited for: 4 -> 16; matrix products, arithmetic and copies ran while one was open for 3% -> 35% of each run, Pallas kernels for 0% -> 8%
where the time goes in v1:
time: 206 us; the launch traced here: 204 us
  waiting for transfers between devices  51.7 us (25%)
  local copies, waits for them, and re-layouts  35.9 us (17%)
  starting transfers between devices  31.5 us (15%)
  other arithmetic  28.6 us (14%)
  blocking collectives  20.4 us (10%)
  matrix products  20.3 us (10%)
  Pallas kernels  15.3 us (7%)
    ppermute x22, waiting for transfers between devices, swap(): lax.ppermute(values, axis, [(i, i ^ 1 << b) for i in range(lax.axis_size(...  39.7 us
    ppermute x22, starting transfers between devices, swap(): lax.ppermute(values, axis, [(i, i ^ 1 << b) for i in range(lax.axis_size(...  23.2 us
    all_to_all x1, blocking collectives, shards(): lax.all_to_all(outgoing, 'sp', split_axis=0, concat_axis=0, tiled=True)  20.4 us
    pallas_call x1, Pallas kernels, shards(): pl.pallas_call(functools.partial(head_kernel, scale_a=(DA + ROPE) ** (-0....  15.3 us
    unnamed x73, local copies, waits for them, and re-layouts  10.5 us
    all_to_all x1, waiting for transfers between devices, shards(): lax.all_to_all(summed.reshape(experts, padded, columns.size), 'sp', split...  8.51 us
    dot_general x1, matrix products, shards(): jnp.dot(act, expert_down[0], preferred_element_type=jnp.float32)  6.41 us
    select_n x13, other arithmetic, join(): jnp.where(low, values, other)  5.99 us
  transfers between devices with their start and end apart: 29, of which 16 were waited for; matrix products, arithmetic and copies ran while one was open for 35% of the time, Pallas kernels for 8%

profile of v1, /device:TPU:0, one launch (start us, length us, event | category | flops | bytes accessed | tf_op | source)
XLA Modules:
  0.0 204.2 jit_solution(10311467265483272540)
XLA Ops:
  1.5 3.1 %collective-permute-start.8 = (bf16[1,96,128]{2,1,0:T(8,128)(2,1)}, bf16[1,96,128]{2,1,0:T(8,128)(2,1)}, u32[]{:S(2)}, u32[]{:S(2)}) collective-permute-start(bf16[1,96,128]{2,1,0:T(8,128)(2,1)} %get-tuple-element.40), channel_id=1, source_target_pairs={{0,8},{4,12},{8,0},{12,4},{16,24},{20,28},{24,16},{28,20},{1,9},{5... | collective-permute-start | bytes 73736 | tf_op jit(solution)/shard_map/ppermute | solution.py:86
  7.7 2.0 collective-permute-start.1
  16.7 1.8 copy.81
  18.5 1.8 copy.88
  21.9 1.8 copy.86
  39.2 2.9 %collective-permute-start.9 = (bf16[2,96,128]{2,1,0:T(8,128)(2,1)S(1)}, bf16[2,96,128]{2,1,0:T(8,128)(2,1)S(1)}, u32[]{:S(2)}, u32[]{:S(2)}) collective-permute-start(bf16[2,96,128]{2,1,0:T(8,128)(2,1)S(1)} %pad_maximum_fusion.24), channel_id=1, source_target_pairs={{0,16},{4,20},{8,24},{12,28},{16,0},{20,4},{24,8},{28,12},{1,17},{... | collective-permute-start | bytes 147464 | tf_op jit(solution)/shard_map/ppermute | solution.py:86
  44.4 2.8 %collective-permute-start.10 = (bf16[4,96,128]{2,1,0:T(8,128)(2,1)S(1)}, bf16[4,96,128]{2,1,0:T(8,128)(2,1)S(1)}, u32[]{:S(2)}, u32[]{:S(2)}) collective-permute-start(bf16[4,96,128]{2,1,0:T(8,128)(2,1)S(1)} %pad_maximum_fusion.21), channel_id=1, source_target_pairs={{0,2},{1,3},{2,0},{3,1},{4,6},{5,7},{6,4},{7,5},{8,10},{9,11},{10,... | collective-permute-start | bytes 294920 | tf_op jit(solution)/shard_map/ppermute | solution.py:86
  47.2 2.6 %collective-permute-done.4 = bf16[2,144,128]{2,1,0:T(8,128)(2,1)S(1)} collective-permute-done((bf16[2,144,128]{2,1,0:T(8,128)(2,1)S(1)}, bf16[2,144,128]{2,1,0:T(8,128)(2,1)S(1)}, u32[]{:S(2)}, u32[]{:S(2)}) %collective-permute-start.4) | collective-permute-done | bytes 73760 | tf_op jit(solution)/shard_map/ppermute | solution.py:86
  52.7 3.0 %collective-permute-done.5 = bf16[4,144,128]{2,1,0:T(8,128)(2,1)S(1)} collective-permute-done((bf16[4,144,128]{2,1,0:T(8,128)(2,1)S(1)}, bf16[4,144,128]{2,1,0:T(8,128)(2,1)S(1)}, u32[]{:S(2)}, u32[]{:S(2)}) %collective-permute-start.5) | collective-permute-done | bytes 147488 | tf_op jit(solution)/shard_map/ppermute | solution.py:86
  60.6 1.9 collective-permute-done.6
  66.8 15.3 %shard_map.190 = bf16[192,1024]{1,0:T(8,128)(2,1)} custom-call(bf16[4,192,128]{2,1,0:T(8,128)(2,1)} %fusion.53.qa_ref, bf16[4,192,256]{2,1,0:T(8,128)(2,1)} %fusion.38.qb_ref, bf16[1536,512]{1,0:T(8,128)(2,1)} %bitcast.64, bf16[1536,128]{1,0:T(8,128)(2,1)} %get-tuple-element.20.rota_ref, bf16[1536,128]{1,0:T(8,128)(2,1)} %get-tuple-element.19.rotb_ref, ...), custom_call_target="tpu_custom_call" | custom-call | tf_op jit(solution)/shard_map/pallas_call | solution.py:167
  82.2 2.0 fusion.4
  92.0 4.1 %collective-permute-done.14 = bf16[192,512]{1,0:T(8,128)(2,1)S(1)} collective-permute-done((bf16[192,512]{1,0:T(8,128)(2,1)S(1)}, bf16[192,512]{1,0:T(8,128)(2,1)S(1)}, u32[]{:S(2)}, u32[]{:S(2)}) %collective-permute-start.14) | collective-permute-done | bytes 196640 | tf_op jit(solution)/shard_map/ppermute | solution.py:86
  103.2 20.4 %all_to_all.10 = bf16[8,72,512]{2,1,0:T(8,128)(2,1)S(1)} all-to-all(bf16[8,72,512]{2,1,0:T(8,128)(2,1)S(1)} %bitcast.76), channel_id=1, replica_groups=mesh['sp'=8,'tp'=4] {'sp'}, dimensions={0} | all-to-all | bytes 1179648 | tf_op jit(solution)/shard_map/all_to_all | solution.py:215
  125.1 11.7 %collective-permute-done.21 = bf16[576,512]{1,0:T(8,128)(2,1)S(1)} collective-permute-done((bf16[576,512]{1,0:T(8,128)(2,1)S(1)}, bf16[576,512]{1,0:T(8,128)(2,1)S(1)}, u32[]{:S(2)}, u32[]{:S(2)}) %collective-permute-start.21) | collective-permute-done | bytes 589856 | tf_op jit(solution)/shard_map/ppermute | solution.py:86
  141.7 2.4 %fusion.8 = f32[576,512]{1,0:T(8,128)} fusion(bf16[1,2048,512]{2,1,0:T(8,128)(2,1)S(1)} %copy-done.29, bf16[576,1024]{1,0:T(8,128)(2,1)S(1)} %get-tuple-element.8, bf16[576,1024]{1,0:T(8,128)(2,1)S(1)} %get-tuple-element.7), kind=kOutput, calls=%fused_computation.9 | convolution fusion | flops 1212678144 | bytes 5636096 | tf_op jit(solution)/shard_map/dot_general | solution.py:225
  144.1 6.4 %convolution_convert_fusion = bf16[576,2048]{1,0:T(8,128)(2,1)} fusion(bf16[1,512,2048]{2,1,0:T(8,128)(2,1)S(1)} %copy-done, f32[576,512]{1,0:T(8,128)} %fusion.8, bf16[1,2048,512]{2,1,0:T(8,128)(2,1)} %param.37, bf16[576,1024]{1,0:T(8,128)(2,1)} %copy-done.8, bf16[576,1024]{1,0:T(8,128)(2,1)S(1)} %get-tuple-element.7), kind=kOutput, calls=%fused_computation.4 | convolution fusion | flops 2423586816 | bytes 10092544 | tf_op jit(solution)/shard_map/dot_general | solution.py:227
  150.5 1.7 broadcast_select_fusion
  161.1 4.9 %fusion.50 = f32[192,2048]{1,0:T(8,128)} fusion(bf16[512,2048]{1,0:T(8,128)(2,1)} %param.36, f32[192,512]{1,0:T(8,128)} %fusion.20, bf16[2048,512]{1,0:T(8,128)(2,1)} %param.34, bf16[192,1024]{1,0:T(8,128)(2,1)} %copy-done.20, bf16[192,1024]{1,0:T(8,128)(2,1)} %copy-done.19), kind=kOutput, calls=%fused_computation.91 | convolution fusion | flops 807469056 | bytes 6946816 | tf_op jit(solution)/shard_map/dot_general | solution.py:221
  166.0 7.7 %collective-permute-done.24 = bf16[576,512]{1,0:T(8,128)(2,1)S(1)} collective-permute-done((bf16[576,512]{1,0:T(8,128)(2,1)S(1)}, bf16[576,512]{1,0:T(8,128)(2,1)S(1)}, u32[]{:S(2)}, u32[]{:S(2)}) %collective-permute-start.24) | collective-permute-done | bytes 589856 | tf_op jit(solution)/shard_map/ppermute | solution.py:86
  173.7 2.8 %add_convert_fusion = bf16[576,512]{1,0:T(8,128)(2,1)} fusion(bf16[576,512]{1,0:T(8,128)(2,1)S(1)} %collective-permute-done.24, f32[576,1024]{1,0:T(8,128)} %copy-done.1, pred[]{:T(512)S(6)} %eq.44), kind=kLoop, calls=%fused_computation.18 | loop fusion | flops 1179648 | bytes 3538945 | tf_op jit(solution)/shard_map/convert_element_type | solution.py:228
  176.5 4.3 %all-to-all-start.1 = ((bf16[8,72,512]{2,1,0:T(8,128)(2,1)}), bf16[8,72,512]{2,1,0:T(8,128)(2,1)S(1)}, u32[]{:S(2)}, u32[]{:S(2)}) async-start(bf16[8,72,512]{2,1,0:T(8,128)(2,1)} %bitcast.23), calls=%async_computation.1 | async-start | bytes 1179648 | tf_op jit(solution)/shard_map/all_to_all | solution.py:229
  187.9 8.5 %all-to-all-done.1 = bf16[8,72,512]{2,1,0:T(8,128)(2,1)S(1)} async-done(((bf16[8,72,512]{2,1,0:T(8,128)(2,1)}), bf16[8,72,512]{2,1,0:T(8,128)(2,1)S(1)}, u32[]{:S(2)}, u32[]{:S(2)}) %all-to-all-start.1) | async-done | bytes 589856 | tf_op jit(solution)/shard_map/all_to_all | solution.py:229
  200.2 2.3 %collective-permute-done.26 = bf16[48,512]{1,0:T(8,128)(2,1)S(1)} collective-permute-done((bf16[48,512]{1,0:T(8,128)(2,1)S(1)}, bf16[48,512]{1,0:T(8,128)(2,1)S(1)}, u32[]{:S(2)}, u32[]{:S(2)}) %collective-permute-start.26) | collective-permute-done | bytes 49184 | tf_op jit(solution)/shard_map/ppermute | solution.py:271
  (215 shorter events, 85.3 us)
Async XLA Ops:
  1.5 36.9 %collective-permute-start.8 = (bf16[1,96,128]{2,1,0:T(8,128)(2,1)}, bf16[1,96,128]{2,1,0:T(8,128)(2,1)}, u32[]{:S(2)}, u32[]{:S(2)}) collective-permute-start(bf16[1,96,128]{2,1,0:T(8,128)(2,1)} %get-tuple-element.40), channel_id=1, source_target_pairs={{0,8},{4,12},{8,0},{12,4},{16,24},{20,28},{24,16},{28,20},{1,9},{5... | collective-permute-start | bytes 73736 | tf_op jit(solution)/shard_map/ppermute | solution.py:86
  6.1 36.0 %collective-permute-start.3 = (bf16[1,144,128]{2,1,0:T(8,128)(2,1)}, bf16[1,144,128]{2,1,0:T(8,128)(2,1)}, u32[]{:S(2)}, u32[]{:S(2)}) collective-permute-start(bf16[1,144,128]{2,1,0:T(8,128)(2,1)} %maximum_bitcast_fusion), channel_id=1, source_target_pairs={{0,8},{4,12},{8,0},{12,4},{16,24},{20,28},{24,16},{28,20},{1,9},{5... | collective-permute-start | bytes 110600 | tf_op jit(solution)/shard_map/ppermute | solution.py:86
  7.7 79.1 %collective-permute-start = (bf16[48,512]{1,0:T(8,128)(2,1)}, bf16[48,512]{1,0:T(8,128)(2,1)}, u32[]{:S(2)}, u32[]{:S(2)}) collective-permute-start(bf16[48,512]{1,0:T(8,128)(2,1)} %get-tuple-element.36), channel_id=1, source_target_pairs={{0,1},{1,0},{2,3},{3,2},{4,5},{5,4},{6,7},{7,6},{8,9},{9,8},{10,11... | collective-permute-start | bytes 147464 | tf_op jit(solution)/shard_map/ppermute | solution.py:271
  7.7 82.7 %collective-permute-start.1 = (bf16[48,512]{1,0:T(8,128)(2,1)}, bf16[48,512]{1,0:T(8,128)(2,1)}, u32[]{:S(2)}, u32[]{:S(2)}) collective-permute-start(bf16[48,512]{1,0:T(8,128)(2,1)} %get-tuple-element.38), channel_id=1, source_target_pairs={{0,2},{1,3},{2,0},{3,1},{4,6},{5,7},{6,4},{7,5},{8,10},{9,11},{10,... | collective-permute-start | bytes 147464 | tf_op jit(solution)/shard_map/ppermute | solution.py:271
  9.7 81.5 %collective-permute-start.2 = (bf16[48,512]{1,0:T(8,128)(2,1)}, bf16[48,512]{1,0:T(8,128)(2,1)}, u32[]{:S(2)}, u32[]{:S(2)}) collective-permute-start(bf16[48,512]{1,0:T(8,128)(2,1)} %get-tuple-element.35), channel_id=1, source_target_pairs={{0,3},{1,2},{2,1},{3,0},{4,7},{5,6},{6,5},{7,4},{8,11},{9,10},{10,... | collective-permute-start | bytes 147464 | tf_op jit(solution)/shard_map/ppermute | solution.py:271
  39.2 5.1 %collective-permute-start.9 = (bf16[2,96,128]{2,1,0:T(8,128)(2,1)S(1)}, bf16[2,96,128]{2,1,0:T(8,128)(2,1)S(1)}, u32[]{:S(2)}, u32[]{:S(2)}) collective-permute-start(bf16[2,96,128]{2,1,0:T(8,128)(2,1)S(1)} %pad_maximum_fusion.24), channel_id=1, source_target_pairs={{0,16},{4,20},{8,24},{12,28},{16,0},{20,4},{24,8},{28,12},{1,17},{... | collective-permute-start | bytes 147464 | tf_op jit(solution)/shard_map/ppermute | solution.py:86
  42.9 6.9 %collective-permute-start.4 = (bf16[2,144,128]{2,1,0:T(8,128)(2,1)S(1)}, bf16[2,144,128]{2,1,0:T(8,128)(2,1)S(1)}, u32[]{:S(2)}, u32[]{:S(2)}) collective-permute-start(bf16[2,144,128]{2,1,0:T(8,128)(2,1)S(1)} %pad_maximum_fusion.23), channel_id=1, source_target_pairs={{0,16},{4,20},{8,24},{12,28},{16,0},{20,4},{24,8},{28,12},{1,17},{... | collective-permute-start | bytes 221192 | tf_op jit(solution)/shard_map/ppermute | solution.py:86
  44.4 7.0 %collective-permute-start.10 = (bf16[4,96,128]{2,1,0:T(8,128)(2,1)S(1)}, bf16[4,96,128]{2,1,0:T(8,128)(2,1)S(1)}, u32[]{:S(2)}, u32[]{:S(2)}) collective-permute-start(bf16[4,96,128]{2,1,0:T(8,128)(2,1)S(1)} %pad_maximum_fusion.21), channel_id=1, source_target_pairs={{0,2},{1,3},{2,0},{3,1},{4,6},{5,7},{6,4},{7,5},{8,10},{9,11},{10,... | collective-permute-start | bytes 294920 | tf_op jit(solution)/shard_map/ppermute | solution.py:86
  49.9 5.8 %collective-permute-start.5 = (bf16[4,144,128]{2,1,0:T(8,128)(2,1)S(1)}, bf16[4,144,128]{2,1,0:T(8,128)(2,1)S(1)}, u32[]{:S(2)}, u32[]{:S(2)}) collective-permute-start(bf16[4,144,128]{2,1,0:T(8,128)(2,1)S(1)} %pad_maximum_fusion.19), channel_id=1, source_target_pairs={{0,4},{4,0},{8,12},{12,8},{16,20},{20,16},{24,28},{28,24},{1,5},{5... | collective-permute-start | bytes 442376 | tf_op jit(solution)/shard_map/ppermute | solution.py:86
  52.2 7.2 %collective-permute-start.11 = (bf16[4,96,256]{2,1,0:T(8,128)(2,1)}, bf16[4,96,256]{2,1,0:T(8,128)(2,1)}, u32[]{:S(2)}, u32[]{:S(2)}) collective-permute-start(bf16[4,96,256]{2,1,0:T(8,128)(2,1)} %pad_maximum_fusion.18), channel_id=1, source_target_pairs={{0,4},{4,0},{8,12},{12,8},{16,20},{20,16},{24,28},{28,24},{1,5},{5... | collective-permute-start | bytes 589832 | tf_op jit(solution)/shard_map/ppermute | solution.py:86
  56.4 6.0 %collective-permute-start.6 = (bf16[8,96,128]{2,1,0:T(8,128)(2,1)}, bf16[8,96,128]{2,1,0:T(8,128)(2,1)}, u32[]{:S(2)}, u32[]{:S(2)}) collective-permute-start(bf16[8,96,128]{2,1,0:T(8,128)(2,1)} %fusion.49), channel_id=1, source_target_pairs={{0,2},{1,3},{2,0},{3,1},{4,6},{5,7},{6,4},{7,5},{8,10},{9,11},{10,... | collective-permute-start | bytes 589832 | tf_op jit(solution)/shard_map/ppermute | solution.py:86
  60.5 4.2 %collective-permute-start.12 = (bf16[8,96,256]{2,1,0:T(8,128)(2,1)S(1)}, bf16[8,96,256]{2,1,0:T(8,128)(2,1)S(1)}, u32[]{:S(2)}, u32[]{:S(2)}) collective-permute-start(bf16[8,96,256]{2,1,0:T(8,128)(2,1)S(1)} %pad_maximum_fusion.12), channel_id=1, source_target_pairs={{0,1},{1,0},{2,3},{3,2},{4,5},{5,4},{6,7},{7,6},{8,9},{9,8},{10,11... | collective-permute-start | bytes 1179656 | tf_op jit(solution)/shard_map/ppermute | solution.py:86
  85.0 2.6 %collective-permute-start.13 = (bf16[192,1024]{1,0:T(8,128)(2,1)}, bf16[192,1024]{1,0:T(8,128)(2,1)}, u32[]{:S(2)}, u32[]{:S(2)}) collective-permute-start(bf16[192,1024]{1,0:T(8,128)(2,1)} %broadcast_select_fusion.11), channel_id=1, source_target_pairs={{0,1},{1,0},{2,3},{3,2},{4,5},{5,4},{6,7},{7,6},{8,9},{9,8},{10,11... | collective-permute-start | bytes 1179656 | tf_op jit(solution)/shard_map/ppermute | solution.py:86
  88.8 7.2 %collective-permute-start.14 = (bf16[192,512]{1,0:T(8,128)(2,1)S(1)}, bf16[192,512]{1,0:T(8,128)(2,1)S(1)}, u32[]{:S(2)}, u32[]{:S(2)}) collective-permute-start(bf16[192,512]{1,0:T(8,128)(2,1)S(1)} %select_convert_fusion.3), channel_id=1, source_target_pairs={{0,2},{1,3},{2,0},{3,1},{4,6},{5,7},{6,4},{7,5},{8,10},{9,11},{10,... | collective-permute-start | bytes 589832 | tf_op jit(solution)/shard_map/ppermute | solution.py:86
  97.5 3.6 %collective-permute-start.16 = (f32[192,1]{0,1:T(1,128)S(1)}, f32[192,1]{0,1:T(1,128)S(1)}, u32[]{:S(2)}, u32[]{:S(2)}) collective-permute-start(f32[192,1]{0,1:T(1,128)S(1)} %add.265), channel_id=1, source_target_pairs={{0,2},{1,3},{2,0},{3,1},{4,6},{5,7},{6,4},{7,5},{8,10},{9,11},{10,... | collective-permute-start | bytes 2312 | tf_op jit(solution)/shard_map/ppermute | solution.py:86
  123.6 13.3 %collective-permute-start.21 = (bf16[576,512]{1,0:T(8,128)(2,1)S(1)}, bf16[576,512]{1,0:T(8,128)(2,1)S(1)}, u32[]{:S(2)}, u32[]{:S(2)}) collective-permute-start(bf16[576,512]{1,0:T(8,128)(2,1)S(1)} %bitcast.68), channel_id=1, source_target_pairs={{0,2},{1,3},{2,0},{3,1},{4,6},{5,7},{6,4},{7,5},{8,10},{9,11},{10,... | collective-permute-start | bytes 1769480 | tf_op jit(solution)/shard_map/ppermute | solution.py:86
  137.2 2.9 %collective-permute-start.22 = (bf16[576,1024]{1,0:T(8,128)(2,1)S(1)}, bf16[576,1024]{1,0:T(8,128)(2,1)S(1)}, u32[]{:S(2)}, u32[]{:S(2)}) collective-permute-start(bf16[576,1024]{1,0:T(8,128)(2,1)S(1)} %pad_maximum_fusion.3), channel_id=1, source_target_pairs={{0,1},{1,0},{2,3},{3,2},{4,5},{5,4},{6,7},{7,6},{8,9},{9,8},{10,11... | collective-permute-start | bytes 3538952 | tf_op jit(solution)/shard_map/ppermute | solution.py:86
  137.3 15.2 %collective-permute-start.17 = (bf16[192,512]{1,0:T(8,128)(2,1)}, bf16[192,512]{1,0:T(8,128)(2,1)}, u32[]{:S(2)}, u32[]{:S(2)}) collective-permute-start(bf16[192,512]{1,0:T(8,128)(2,1)} %fusion.34), channel_id=1, source_target_pairs={{0,2},{1,3},{2,0},{3,1},{4,6},{5,7},{6,4},{7,5},{8,10},{9,11},{10,... | collective-permute-start | bytes 589832 | tf_op jit(solution)/shard_map/ppermute | solution.py:86
  152.3 3.7 %collective-permute-start.23 = (bf16[576,1024]{1,0:T(8,128)(2,1)S(1)}, bf16[576,1024]{1,0:T(8,128)(2,1)S(1)}, u32[]{:S(2)}, u32[]{:S(2)}) collective-permute-start(bf16[576,1024]{1,0:T(8,128)(2,1)S(1)} %broadcast_select_fusion), channel_id=1, source_target_pairs={{0,1},{1,0},{2,3},{3,2},{4,5},{5,4},{6,7},{7,6},{8,9},{9,8},{10,11... | collective-permute-start | bytes 3538952 | tf_op jit(solution)/shard_map/ppermute | solution.py:86
  158.2 15.6 %collective-permute-start.24 = (bf16[576,512]{1,0:T(8,128)(2,1)S(1)}, bf16[576,512]{1,0:T(8,128)(2,1)S(1)}, u32[]{:S(2)}, u32[]{:S(2)}) collective-permute-start(bf16[576,512]{1,0:T(8,128)(2,1)S(1)} %select_convert_fusion), channel_id=1, source_target_pairs={{0,2},{1,3},{2,0},{3,1},{4,6},{5,7},{6,4},{7,5},{8,10},{9,11},{10,... | collective-permute-start | bytes 1769480 | tf_op jit(solution)/shard_map/ppermute | solution.py:86
  176.5 19.8 %all-to-all-start.1 = ((bf16[8,72,512]{2,1,0:T(8,128)(2,1)}), bf16[8,72,512]{2,1,0:T(8,128)(2,1)S(1)}, u32[]{:S(2)}, u32[]{:S(2)}) async-start(bf16[8,72,512]{2,1,0:T(8,128)(2,1)} %bitcast.23), calls=%async_computation.1 | async-start | bytes 1179648 | tf_op jit(solution)/shard_map/all_to_all | solution.py:229
  186.3 10.4 %collective-permute-start.20 = (bf16[192,512]{1,0:T(8,128)(2,1)}, bf16[192,512]{1,0:T(8,128)(2,1)}, u32[]{:S(2)}, u32[]{:S(2)}) collective-permute-start(bf16[192,512]{1,0:T(8,128)(2,1)} %select_convert_fusion.2), channel_id=1, source_target_pairs={{0,2},{1,3},{2,0},{3,1},{4,6},{5,7},{6,4},{7,5},{8,10},{9,11},{10,... | collective-permute-start | bytes 589832 | tf_op jit(solution)/shard_map/ppermute | solution.py:86
  198.3 4.2 %collective-permute-start.26 = (bf16[48,512]{1,0:T(8,128)(2,1)S(1)}, bf16[48,512]{1,0:T(8,128)(2,1)S(1)}, u32[]{:S(2)}, u32[]{:S(2)}) collective-permute-start(bf16[48,512]{1,0:T(8,128)(2,1)S(1)} %get-tuple-element.32), channel_id=1, source_target_pairs={{0,2},{1,3},{2,0},{3,1},{4,6},{5,7},{6,4},{7,5},{8,10},{9,11},{10,... | collective-permute-start | bytes 147464 | tf_op jit(solution)/shard_map/ppermute | solution.py:271
  199.9 3.7 %collective-permute-start.27 = (bf16[48,512]{1,0:T(8,128)(2,1)S(1)}, bf16[48,512]{1,0:T(8,128)(2,1)S(1)}, u32[]{:S(2)}, u32[]{:S(2)}) collective-permute-start(bf16[48,512]{1,0:T(8,128)(2,1)S(1)} %get-tuple-element.31), channel_id=1, source_target_pairs={{0,3},{1,2},{2,1},{3,0},{4,7},{5,6},{6,5},{7,4},{8,11},{9,10},{10,... | collective-permute-start | bytes 147464 | tf_op jit(solution)/shard_map/ppermute | solution.py:271
  (36 other events, 354.1 us)
